TPU v7x, 32 devices: a whole 2x2x4 slice. The times are simulated.
32 devices in a mesh: grp: 2 (over x), ep: 8 (over z, y), tp: 2 (over core).
Axes of the slice: x: 2, y: 2, z: 4, core: 2. Of those that a mesh axis runs over, the one named last changes fastest.
Arguments:
- tokens: bfloat16 [2304, 2048], P(('grp', 'ep')), parts along dimension 0, may hold values from -6 to 6
- norm_gain: bfloat16 [2048], replicated, may hold values from 0.099609375 to 1.8984375
- chosen_rows: int32 [16, 144], P('grp', 'ep'), parts along dimension 0, may hold values from 0 to 1151, as said below
- route_weights: float32 [16, 144], P('grp', 'ep'), parts along dimension 0, may hold values from 0.2 to 1
- gate_weight: bfloat16 [8, 2048, 1536], P('ep', None, 'tp'), may hold values from -0.125 to 0.125
- up_weight: bfloat16 [8, 2048, 1536], P('ep', None, 'tp'), may hold values from -0.125 to 0.125
- down_weight: bfloat16 [8, 1536, 2048], P('ep', 'tp'), may hold values from -0.15625 to 0.15625
Outputs:
- mixed: bfloat16 [2304, 2048], P(('grp', 'ep', 'tp')), parts along dimension 0
There are 2 independent parts, one for each index of `grp`. A program takes and returns all parts, laid end to end along the dimension named above; an argument that names none is the same for every part. Nothing has to cross between parts.
Inputs may be any that keep to these rules, and one draw needn't show every extreme that they name: `chosen_rows`: the columns come in blocks of 18, one block for each index of ep's 144 tokens in order. In every row the first half of a block names distinct tokens of the first half of that block's tokens, and its second half distinct tokens of the second half.
All inputs are finite; a program needn't handle non-finite values.
Results may differ from a plain program's by a relative error of at most 0.01.
Values may be sent and summed in bfloat16 or wider, within the bound.
A program may use at most 128 MiB of HBM per device.

v0:
```python
import jax
import jax.numpy as jnp
from jax import lax
from jax.sharding import PartitionSpec as P


def rms_apply(values_in, norm_gain):
    values = values_in.astype(jnp.float32)
    scale = lax.rsqrt(jnp.mean(values * values, axis=-1, keepdims=True) + 1e-06)
    return (values * scale * norm_gain.astype(jnp.float32)).astype(jnp.bfloat16)


def local(tokens, norm_gain, chosen_rows, route_weights, gate_weight, up_weight, down_weight):
    tok_rows = tokens.shape[0]
    width = tokens.shape[1]
    experts = chosen_rows.shape[0]
    slots = chosen_rows.shape[1]
    half_slots = slots // 2
    half_rows = tok_rows // 2
    source_id = lax.axis_index("ep")
    core_id = lax.axis_index("tp")
    local_rows = (chosen_rows - source_id * tok_rows).reshape(experts, 2, half_slots)
    source_rows = rms_apply(tokens, norm_gain)
    own_half = lax.dynamic_index_in_dim(local_rows, core_id, 1, keepdims=False)
    outgoing = source_rows[own_half]
    received = lax.all_to_all(outgoing, "ep", split_axis=0, concat_axis=0, tiled=True)
    arrived = lax.all_gather(received[None], "tp", axis=0, tiled=True)
    expert_in = arrived.reshape(-1, width)
    gate_proj = jnp.dot(expert_in, gate_weight[0], preferred_element_type=jnp.float32)
    up_proj = jnp.dot(expert_in, up_weight[0], preferred_element_type=jnp.float32)
    hidden = (jax.nn.silu(gate_proj) * up_proj).astype(jnp.bfloat16)
    summed = lax.psum_scatter(
        jnp.dot(hidden, down_weight[0], preferred_element_type=jnp.float32).astype(jnp.bfloat16),
        "tp",
        scatter_dimension=0,
        tiled=True,
    )
    expert_out = summed.reshape(experts, half_slots, width)
    results = lax.all_to_all(expert_out, "ep", split_axis=0, concat_axis=0, tiled=True)
    row_index = (
        lax.dynamic_index_in_dim(local_rows, core_id, 1, keepdims=False) - core_id * half_rows
    )
    weight_half = lax.dynamic_index_in_dim(
        route_weights.reshape(experts, 2, half_slots), core_id, 1, keepdims=False
    )
    contrib = weight_half.reshape(-1, 1) * results.reshape(-1, width).astype(jnp.float32)
    mixed = jnp.zeros((half_rows, width), jnp.float32).at[row_index.reshape(-1)].add(contrib)
    return mixed.astype(jnp.bfloat16)


def solution(mesh):
    return jax.shard_map(
        local,
        mesh=mesh,
        in_specs=(
            P(("grp", "ep"), None),
            P(),
            P("grp", "ep"),
            P("grp", "ep"),
            P("ep", None, "tp"),
            P("ep", None, "tp"),
            P("ep", "tp", None),
        ),
        out_specs=P(("grp", "ep", "tp"), None),
        check_vma=False,
    )
```

profile of v0, /device:TPU:0, one launch (start us, length us, event | category | flops | bytes accessed | tf_op | source)
XLA Modules:
  0.0 93.9 jit_solution(9900520229802952924)
XLA Ops:
  6.5 0.0 copy-start
  6.5 0.0 reduce-scatter.2.cloned.1.call-start
  6.5 1.4 %fusion.15 = f32[144]{0:T(256)S(1)} fusion(bf16[144,2048]{1,0:T(8,128)(2,1)} %param.7), kind=kLoop, calls=%fused_computation.13 | loop fusion | flops 884592 | bytes 590400 | tf_op jit(solution)/shard_map/reduce_sum | solution.py:9
  8.0 0.7 broadcast_subtract_fusion
  8.7 0.1 reshape.78
  8.8 0.1 reshape.85
  8.9 0.7 convert_element_type.25
  9.6 2.1 %fusion.17 = bf16[144,2048]{1,0:T(8,128)(2,1)} fusion(bf16[144,2048]{1,0:T(8,128)(2,1)} %param.7, f32[2048]{0:T(1024)S(1)} %convert_element_type.25, f32[144]{0:T(256)S(1)} %add_rsqrt_fusion), kind=kLoop, calls=%fused_computation.15 | loop fusion | flops 1179648 | bytes 1188416 | tf_op jit(solution)/shard_map/convert_element_type | solution.py:10
  11.6 2.2 %gather_fusion = bf16[72,2048]{1,0:T(8,128)(2,1)S(1)} fusion(bf16[144,2048]{1,0:T(8,128)(2,1)} %fusion.17, s32[1024]{0:T(1024)S(1)} %pad_clamp_fusion), kind=kCustom, calls=%fused_computation | custom fusion | bytes 590112 | tf_op jit(solution)/shard_map/gather | solution.py:25
  13.8 0.9 reshape.84
  14.7 21.8 %all_to_all.10 = bf16[8,9,2048]{2,1,0:T(8,128)(2,1)S(1)} all-to-all(bf16[8,9,2048]{2,1,0:T(8,128)(2,1)} %reshape.84), channel_id=1, replica_groups=mesh['grp'=2,'ep'=8,'tp'=2] {'ep'}, dimensions={0} | all-to-all | bytes 589824 | tf_op jit(solution)/shard_map/all_to_all | solution.py:26
  36.6 0.2 copy.11
  36.8 2.2 %all-gather = bf16[16,9,2048]{2,0,1:T(8,128)(2,1)S(1)} all-gather(bf16[8,9,2048]{2,0,1:T(8,128)(2,1)S(1)} %copy.11), channel_id=2, replica_groups=mesh['grp'=2,'ep'=8,'tp'=2] {'tp'}, dimensions={0}, use_global_device_ids=true | all-gather | bytes 884736 | tf_op jit(solution)/shard_map/all_gather | solution.py:27
  39.0 1.4 %copy.12 = bf16[16,9,2048]{2,1,0:T(8,128)(2,1)} copy(bf16[16,9,2048]{2,0,1:T(8,128)(2,1)S(1)} %all-gather) | data formatting | bytes 1179648 | tf_op jit(solution)/shard_map/all_gather | solution.py:27
  40.4 2.3 %reshape.80 = bf16[144,2048]{1,0:T(8,128)(2,1)} reshape(bf16[16,9,2048]{2,1,0:T(8,128)(2,1)} %copy.12) | data formatting | bytes 1179648 | tf_op jit(solution)/shard_map/reshape | solution.py:28
  42.7 3.5 %fusion.4 = f32[144,768]{1,0:T(8,128)} fusion(bf16[144,2048]{1,0:T(8,128)(2,1)} %reshape.80, bf16[1,2048,768]{2,1,0:T(8,128)(2,1)} %param.11), kind=kOutput, calls=%fused_computation.6 | convolution fusion | flops 452984832 | bytes 4177920 | tf_op jit(solution)/shard_map/dot_general | solution.py:29
  46.2 0.0 copy-done
  46.2 0.0 copy-start.1
  46.2 4.3 %fusion.6 = bf16[144,2048]{1,0:T(8,128)(2,1)} fusion(bf16[1,768,2048]{2,1,0:T(8,128)(2,1)S(1)} %copy-done, bf16[144,2048]{1,0:T(8,128)(2,1)} %reshape.80, bf16[1,2048,768]{2,1,0:T(8,128)(2,1)} %param.12, f32[144,768]{1,0:T(8,128)} %fusion.4), kind=kOutput, calls=%fused_computation.8 | convolution fusion | flops 906928128 | bytes 7913472 | tf_op jit(solution)/shard_map/dot_general | solution.py:33
  50.5 0.0 reduce-scatter.2.cloned.1.call-update
  50.5 7.2 %reduce-scatter.2.cloned.1.call-done = bf16[72,2048]{1,0:T(8,128)(2,1)} async-done(((bf16[144,2048]{1,0:T(8,128)(2,1)}), bf16[72,2048]{1,0:T(8,128)(2,1)}) %reduce-scatter.2.cloned.1.call-update) | async-done | bytes 294928 | tf_op jit(solution)/shard_map/reduce_scatter | solution.py:32
  57.6 1.9 %reshape.81 = bf16[8,9,2048]{2,1,0:T(8,128)(2,1)} reshape(bf16[72,2048]{1,0:T(8,128)(2,1)} %reduce-scatter.2.cloned.1.call-done) | data formatting | bytes 589824 | tf_op jit(solution)/shard_map/reshape | solution.py:38
  59.5 5.7 %all-to-all-start.1 = ((bf16[8,9,2048]{2,1,0:T(8,128)(2,1)}), bf16[8,9,2048]{2,1,0:T(8,128)(2,1)}, u32[]{:S(2)}, u32[]{:S(2)}) async-start(bf16[8,9,2048]{2,1,0:T(8,128)(2,1)} %reshape.81), calls=%async_computation.2 | async-start | bytes 1048576 | tf_op jit(solution)/shard_map/all_to_all | solution.py:39
  65.2 0.1 sub.27
  65.3 0.0 copy-done.1
  65.3 0.1 reshape.79
  65.4 0.1 mul.44
  65.5 14.8 %all-to-all-done.1 = bf16[8,9,2048]{2,1,0:T(8,128)(2,1)} async-done(((bf16[8,9,2048]{2,1,0:T(8,128)(2,1)}), bf16[8,9,2048]{2,1,0:T(8,128)(2,1)}, u32[]{:S(2)}, u32[]{:S(2)}) %all-to-all-start.1) | async-done | bytes 294944 | tf_op jit(solution)/shard_map/all_to_all | solution.py:39
  80.3 2.0 %reshape.82 = f32[72,2048]{1,0:T(8,128)} reshape(bf16[8,9,2048]{2,1,0:T(8,128)(2,1)} %all-to-all-done.1) | data formatting | bytes 884736 | tf_op jit(solution)/shard_map/convert_element_type | solution.py:46
  82.3 2.9 %scatter_custom_fusion = f32[72,2048]{1,0:T(8,128)} fusion(s32[72]{0:T(128)S(1)} %fusion.30, f32[72,2048]{1,0:T(8,128)} %reshape.82, f32[72]{0:T(128)S(1)} %mul.44, f32[]{:T(128)} %constant.11.clone.1), kind=kCustom, calls=%fused_computation.16 | custom fusion | flops 294912 | bytes 1180164 | tf_op jit(solution)/shard_map/scatter-add | solution.py:47
  85.2 1.8 %convert_element_type.31 = bf16[72,2048]{1,0:T(8,128)(2,1)} convert(f32[72,2048]{1,0:T(8,128)} %scatter_custom_fusion) | non-fusion elementwise | flops 147456 | bytes 884736 | tf_op jit(solution)/shard_map/convert_element_type | solution.py:48
  (6 shorter events, 0.1 us)
Async XLA Ops:
  6.5 39.6 %copy-start = (bf16[1,768,2048]{2,1,0:T(8,128)(2,1)S(1)}, bf16[1,768,2048]{2,1,0:T(8,128)(2,1)}, u32[]{:S(2)}) copy-start(bf16[1,768,2048]{2,1,0:T(8,128)(2,1)} %param.13) | copy-start | bytes 9437188
  6.5 51.1 %reduce-scatter.2.cloned.1.call-start = ((), (), s32[]{:S(2)}) async-start(), calls=%async_computation.3 | async-start | bytes 884736 | tf_op jit(solution)/shard_map/reduce_scatter | solution.py:32
  46.2 19.2 %copy-start.1 = (f32[8,18]{1,0:T(8,128)S(1)}, f32[8,18]{1,0:T(8,128)}, u32[]{:S(2)}) copy-start(f32[8,18]{1,0:T(8,128)} %param.10) | copy-start | bytes 1732
  59.5 20.8 %all-to-all-start.1 = ((bf16[8,9,2048]{2,1,0:T(8,128)(2,1)}), bf16[8,9,2048]{2,1,0:T(8,128)(2,1)}, u32[]{:S(2)}, u32[]{:S(2)}) async-start(bf16[8,9,2048]{2,1,0:T(8,128)(2,1)} %reshape.81), calls=%async_computation.2 | async-start | bytes 1048576 | tf_op jit(solution)/shard_map/all_to_all | solution.py:39
Sparse Core Ops, SparseCore 0:
  50.6 6.9 reduce-scatter.1
where the time goes:
time: 94.5 us; the launch traced here: 93.9 us
  blocking collectives  24.1 us (26%)
  waiting for transfers between devices  22 us (23%)
  between operations  13.4 us (14%)
  local copies, waits for them, and re-layouts  11.2 us (12%)
  other arithmetic  9.62 us (10%)
  matrix products  7.79 us (8%)
  starting transfers between devices  5.73 us (6%)
    all_to_all x1, blocking collectives, local(): lax.all_to_all(outgoing, 'ep', split_axis=0, concat_axis=0, tiled=True)  21.8 us
    all_to_all x1, waiting for transfers between devices, local(): lax.all_to_all(expert_out, 'ep', split_axis=0, concat_axis=0, tiled=True)  14.8 us
    reduce_scatter x1, waiting for transfers between devices, local(): lax.psum_scatter(jnp.dot(hidden, down_weight[0], preferred_element_type=j...  7.16 us
    all_to_all x1, starting transfers between devices, local(): lax.all_to_all(expert_out, 'ep', split_axis=0, concat_axis=0, tiled=True)  5.72 us
    dot_general x1, matrix products, local(): jnp.dot(hidden, down_weight[0], preferred_element_type=jnp.float32)  4.3 us
    dot_general x1, matrix products, local(): jnp.dot(expert_in, gate_weight[0], preferred_element_type=jnp.float32)  3.49 us
    gather x2, local copies, waits for them, and re-layouts, local(): outgoing = source_rows[own_half]  3.1 us
    scatter-add x1, other arithmetic, local(): jnp.zeros((half_rows, width), jnp.float32).at[row_index.reshape(-1)]  2.89 us
  transfers between devices with their start and end apart: 2, of which 2 were waited for; matrix products, arithmetic and copies ran while one was open for 0% of the time, Pallas kernels for 0%

commit v1 on v0

v1 whole, which is shorter than its diff:
```python
import functools

import jax
import jax.numpy as jnp
from jax import lax
from jax.experimental import pallas as pl
from jax.experimental.pallas import tpu as pltpu
from jax.sharding import PartitionSpec as P

MESH = pl.DeviceIdType.MESH
LANES = 128
SUB = 8
GROUP = 8


def loop(count, body):
    if count == 1:
        body(0)
    else:
        lax.fori_loop(0, count, lambda i, carry: (body(i), carry)[1], 0)


def kernel(
    n,
    tokens,
    gain,
    chosen,
    route,
    gate_w,
    up_w,
    down_w,
    mixed,
    tok,
    wg,
    wu,
    wd,
    normed,
    out_x,
    in_x,
    sib_x,
    flat,
    x_cols,
    gate_acc,
    up_acc,
    hidden,
    p_send,
    p_recv,
    p_own,
    c_send,
    c_recv,
    g_rows,
    w_rows,
    r_cols,
    load_sem,
    d_send,
    d_recv,
    f_send,
    f_recv,
    q_send,
    q_recv,
    b_send,
    b_recv,
):
    chunks = out_x.shape[0]
    half_rows, width = tok.shape
    experts, slots = chosen.shape
    half = slots // 2
    rows = experts * half
    block = GROUP * half
    blocks = rows // block
    cols = width // chunks
    me = lax.axis_index("ep")
    core = lax.axis_index("tp")
    sib = {"tp": 1 - core}

    def peer(i):
        return lax.rem(me + i, n)

    barrier = pltpu.get_barrier_semaphore()
    pl.semaphore_signal(barrier, inc=1, device_id=sib, device_id_type=MESH)
    lax.fori_loop(
        1,
        n,
        lambda i, c: (
            pl.semaphore_signal(barrier, inc=1, device_id={"ep": peer(i)}, device_id_type=MESH),
            c,
        )[1],
        0,
    )
    base = pl.multiple_of(core * half_rows, 8)
    load_tok = pltpu.make_async_copy(tokens.at[pl.ds(base, half_rows)], tok, load_sem.at[0])
    load_tok.start()
    loads = [
        pltpu.make_async_copy(src.at[0], dst, load_sem.at[i + 1])
        for i, (src, dst) in enumerate(((gate_w, wg), (up_w, wu), (down_w, wd)))
    ]
    for load in loads:
        load.start()
    load_tok.wait()

    g = gain[...].astype(jnp.float32)
    values = tok[...].astype(jnp.float32)
    scale = lax.rsqrt(jnp.mean(values * values, axis=-1, keepdims=True) + 1e-06)
    normed[...] = (values * scale * g).astype(jnp.bfloat16)

    first = me * (2 * half_rows) + core * half_rows
    picked = (chosen[...] - first).astype(jnp.float32).T
    weight = route[...].T
    lane = lax.broadcasted_iota(jnp.int32, (half, half_rows), 1).astype(jnp.float32)
    for e in range(experts):
        pair = [picked[h * half : (h + 1) * half, e : e + 1] for h in range(2)]
        row = jnp.where(core == 0, pair[0], pair[1])
        pair = [weight[h * half : (h + 1) * half, e : e + 1] for h in range(2)]
        share = jnp.where(core == 0, pair[0], pair[1])
        here = lane == row
        g_rows[e * half : (e + 1) * half, :] = jnp.where(here, 1.0, 0.0)
        w_rows[e * half : (e + 1) * half, :] = jnp.where(here, share, 0.0)

    def start_of(b):
        return b * block if isinstance(b, int) else pl.multiple_of(b * block, 8)

    def pack(value, ref, j, b):
        for s in range(SUB):
            flat[pl.ds(s, block, stride=SUB), :] = value[:, s * LANES : (s + 1) * LANES]
        ref[j, pl.ds(b * block, block)] = (
            flat[: block * SUB, :].reshape(block, SUB, LANES).astype(jnp.bfloat16)
        )

    def gather(j):
        def one(b):
            hot = g_rows[pl.ds(start_of(b), block), :].astype(jnp.bfloat16)
            got = jnp.dot(
                hot, normed[:, j * cols : (j + 1) * cols], preferred_element_type=jnp.float32
            )
            pack(got, out_x, j, b)

        loop(blocks, one)

    def mine(ref, j, e):
        return ref.at[j, pl.ds(e * half, half)]

    def exchange(src, dst, j, send_sem, recv_sem):
        def one(i, c):
            e = peer(i)
            pltpu.make_async_remote_copy(
                src_ref=mine(src, j, e),
                dst_ref=mine(dst, j, me),
                send_sem=send_sem.at[j],
                recv_sem=recv_sem.at[j],
                device_id={"ep": e},
                device_id_type=MESH,
            ).start()
            return c

        lax.fori_loop(1, n, one, 0)
        for r in range(half):
            dst[j, me * half + r] = src[j, me * half + r]

    def all_of(src, dst, j, send_sem, recv_sem):
        part = pl.ds(0, (n - 1) * half)
        return pltpu.make_async_remote_copy(
            src_ref=src.at[j, part],
            dst_ref=dst.at[j, part],
            send_sem=send_sem.at[j],
            recv_sem=recv_sem.at[j],
            device_id=sib,
            device_id_type=MESH,
        )

    def to_sib(src, dst, j, send_sem, recv_sem):
        return pltpu.make_async_remote_copy(
            src_ref=src.at[j],
            dst_ref=dst.at[j],
            send_sem=send_sem.at[j],
            recv_sem=recv_sem.at[j],
            device_id=sib,
            device_id_type=MESH,
        )

    gather(0)
    pl.semaphore_wait(barrier, n)
    exchange(out_x, in_x, 0, d_send, d_recv)
    for j in range(1, chunks):
        gather(j)
        exchange(out_x, in_x, j, d_send, d_recv)

    for j in range(chunks):
        all_of(out_x, in_x, j, d_send, d_recv).wait_recv()
        to_sib(in_x, sib_x, j, f_send, f_recv).start()
    for load in loads:
        load.wait()
    for j in range(chunks):
        to_sib(in_x, sib_x, j, f_send, f_recv).wait_recv()

        def project(b):
            for h, ref in enumerate((in_x, sib_x)):
                got = ref[j, pl.ds(b * block, block)].astype(jnp.float32)
                flat[pl.ds(h * block * SUB, block * SUB), :] = got.reshape(block * SUB, LANES)
            for s in range(SUB):
                x_cols[:, s * LANES : (s + 1) * LANES] = flat[
                    pl.ds(s, 2 * block, stride=SUB), :
                ].astype(jnp.bfloat16)
            x = x_cols[...]
            depth = slice(j * cols, (j + 1) * cols)
            gate = jnp.dot(x, wg[depth, :], preferred_element_type=jnp.float32)
            up = jnp.dot(x, wu[depth, :], preferred_element_type=jnp.float32)
            if j > 0:
                gate = gate + gate_acc[b]
                up = up + up_acc[b]
            if j < chunks - 1:
                gate_acc[b] = gate
                up_acc[b] = up
            else:
                hidden[b] = (gate / (1.0 + jnp.exp(-gate)) * up).astype(jnp.bfloat16)

        loop(blocks, project)

    for j in range(chunks):

        def down(b):
            part = jnp.dot(
                hidden[b], wd[:, j * cols : (j + 1) * cols], preferred_element_type=jnp.float32
            )
            p_own[j, b] = part[:block].astype(jnp.bfloat16)
            p_send[j, b] = part[block:].astype(jnp.bfloat16)

        loop(blocks, down)
        to_sib(p_send, p_recv, j, q_send, q_recv).start()

    for j in range(chunks):
        to_sib(p_send, p_recv, j, q_send, q_recv).wait_recv()

        def combine(b):
            total = p_own[j, b].astype(jnp.float32) + p_recv[j, b].astype(jnp.float32)
            pack(total, c_send, j, b)

        loop(blocks, combine)
        exchange(c_send, c_recv, j, b_send, b_recv)

    spread = w_rows[...].T
    high = spread.astype(jnp.bfloat16)
    low = (spread - high.astype(jnp.float32)).astype(jnp.bfloat16)
    for j in range(chunks):
        all_of(c_send, c_recv, j, b_send, b_recv).wait_recv()

        def unpack(b):
            got = c_recv[j, pl.ds(b * block, block)].astype(jnp.float32)
            flat[: block * SUB, :] = got.reshape(block * SUB, LANES)
            at = start_of(b)
            for s in range(SUB):
                r_cols[pl.ds(at, block), s * LANES : (s + 1) * LANES] = flat[
                    pl.ds(s, block, stride=SUB), :
                ]

        loop(blocks, unpack)
        res = r_cols[...].astype(jnp.bfloat16)
        total = jnp.dot(high, res, preferred_element_type=jnp.float32)
        total = total + jnp.dot(low, res, preferred_element_type=jnp.float32)
        mixed[:, j * cols : (j + 1) * cols] = total.astype(jnp.bfloat16)

    for j in range(chunks):
        all_of(out_x, in_x, j, d_send, d_recv).wait_send()
        to_sib(in_x, sib_x, j, f_send, f_recv).wait_send()
        to_sib(p_send, p_recv, j, q_send, q_recv).wait_send()
        all_of(c_send, c_recv, j, b_send, b_recv).wait_send()


def local(n, tokens, norm_gain, chosen_rows, route_weights, gate_weight, up_weight, down_weight):
    tok_rows, width = tokens.shape
    half_rows = tok_rows // 2
    experts, slots = chosen_rows.shape
    half = slots // 2
    rows = experts * half
    block = GROUP * half
    blocks = rows // block
    ff = gate_weight.shape[2]
    chunks = width // (LANES * SUB)
    cols = width // chunks
    bf16, f32 = jnp.bfloat16, jnp.float32
    packed = pltpu.VMEM((chunks, rows, SUB, LANES), bf16)
    partial = pltpu.VMEM((chunks, blocks, block, cols), bf16)
    vmem = pl.BlockSpec(memory_space=pltpu.VMEM)
    hbm = pl.BlockSpec(memory_space=pl.ANY)
    return pl.pallas_call(
        functools.partial(kernel, n),
        out_shape=jax.ShapeDtypeStruct((half_rows, width), bf16),
        in_specs=[hbm, vmem, vmem, vmem, hbm, hbm, hbm],
        out_specs=vmem,
        scratch_shapes=[
            pltpu.VMEM((half_rows, width), bf16),
            pltpu.VMEM(gate_weight.shape[1:], bf16),
            pltpu.VMEM(up_weight.shape[1:], bf16),
            pltpu.VMEM(down_weight.shape[1:], bf16),
            pltpu.VMEM((half_rows, width), bf16),
            packed,
            packed,
            packed,
            pltpu.VMEM((2 * block * SUB, LANES), f32),
            pltpu.VMEM((2 * block, cols), bf16),
            pltpu.VMEM((blocks, 2 * block, ff), f32),
            pltpu.VMEM((blocks, 2 * block, ff), f32),
            pltpu.VMEM((blocks, 2 * block, ff), bf16),
            partial,
            partial,
            partial,
            packed,
            packed,
            pltpu.VMEM((rows, half_rows), f32),
            pltpu.VMEM((rows, half_rows), f32),
            pltpu.VMEM((rows, cols), f32),
            pltpu.SemaphoreType.DMA((4,)),
        ]
        + [pltpu.SemaphoreType.DMA((chunks,))] * 8,
        compiler_params=pltpu.CompilerParams(
            collective_id=0, has_side_effects=True, vmem_limit_bytes=60 * 1024 * 1024
        ),
    )(
        tokens,
        norm_gain.reshape(1, width),
        chosen_rows,
        route_weights,
        gate_weight,
        up_weight,
        down_weight,
    )


def solution(mesh):
    return jax.shard_map(
        functools.partial(local, mesh.shape["ep"]),
        mesh=mesh,
        in_specs=(
            P(("grp", "ep"), None),
            P(),
            P("grp", "ep"),
            P("grp", "ep"),
            P("ep", None, "tp"),
            P("ep", None, "tp"),
            P("ep", "tp", None),
        ),
        out_specs=P(("grp", "ep", "tp"), None),
        check_vma=False,
    )
```

time: 94.5 us -> 30.1 us (0.32)
  Pallas kernels: 0 us -> 26.9 us
  blocking collectives: 24.1 us -> 0 us
  waiting for transfers between devices: 22 us -> 0 us
  between operations: 13.4 us -> 0.01 us
  other arithmetic: 9.62 us -> 0 us
  local copies, waits for them, and re-layouts: 11.2 us -> 2.98 us
  matrix products: 7.79 us -> 0 us
  starting transfers between devices: 5.73 us -> 0 us
    pallas_call x0 -> x1, Pallas kernels: none -> 26.9 us  [local(): pl.pallas_call(functools.partial(kernel, n), out_shape=jax.ShapeDtypeStru...]
    all_to_all x1 -> x0, blocking collectives: 21.8 us -> none  [local(): lax.all_to_all(outgoing, 'ep', split_axis=0, concat_axis=0, tiled=True)]
    all_to_all x1 -> x0, waiting for transfers between devices: 14.8 us -> none  [local(): lax.all_to_all(expert_out, 'ep', split_axis=0, concat_axis=0, tiled=True)]
    dot_general x2 -> x0, matrix products: 7.79 us -> none  [the longest x1 4.3 us: local(): jnp.dot(hidden, down_weight[0], preferred_element_type=jnp.float32)]
    reduce_scatter x1 -> x0, waiting for transfers between devices: 7.16 us -> none  [local(): lax.psum_scatter(jnp.dot(hidden, down_weight[0], preferred_element_type=j...]
    all_to_all x1 -> x0, starting transfers between devices: 5.72 us -> none  [local(): lax.all_to_all(expert_out, 'ep', split_axis=0, concat_axis=0, tiled=True)]
    convert_element_type x3 -> x0, other arithmetic: 4.57 us -> none  [the longest x2 2.76 us: rms_apply(): return (values * scale * norm_gain.astype(jnp.float32)).astype(jnp.bfloat16)]
    gather x2 -> x0, local copies, waits for them, and re-layouts: 3.1 us -> none  [local(): outgoing = source_rows[own_half]]
  transfers between devices with their start and end apart: 2 -> 0, of which waited for: 2 -> 0; matrix products, arithmetic and copies ran while one was open for 0% -> 0% of each run, Pallas kernels for 0% -> 0%
where the time goes in v1:
time: 30.1 us; the launch traced here: 29.9 us
  Pallas kernels  26.9 us (89%)
  local copies, waits for them, and re-layouts  2.98 us (10%)
    pallas_call x1, Pallas kernels, local(): pl.pallas_call(functools.partial(kernel, n), out_shape=jax.ShapeDtypeStru...  26.9 us
    unnamed x1, local copies, waits for them, and re-layouts  1.69 us
    reshape x1, local copies, waits for them, and re-layouts, local(): norm_gain.reshape(1, width)  1.29 us

profile of v1, /device:TPU:0, one launch (start us, length us, event | category | flops | bytes accessed | tf_op | source)
XLA Modules:
  0.0 29.9 jit_solution(15505143011974176455)
XLA Ops:
  0.0 1.3 %reshape.3.gain = bf16[1,2048]{1,0:T(2,128)(2,1)} reshape(bf16[2048]{0:T(1024)(128)(2,1)} %param.8) | data formatting | bytes 8192 | tf_op jit(solution)/shard_map/reshape | solution.py:319
  1.3 26.9 %shard_map.73 = bf16[72,2048]{1,0:T(8,128)(2,1)} custom-call(bf16[144,2048]{1,0:T(8,128)(2,1)} %tokens.1, bf16[1,2048]{1,0:T(2,128)(2,1)} %reshape.3.gain, s32[8,18]{1,0:T(8,128)} %chosen.1, f32[8,18]{1,0:T(8,128)} %route.1, bf16[1,2048,768]{2,1,0:T(8,128)(2,1)} %gate_w.1, bf16[1,2048,768]{2,1,0:T(8,128)(2,1)} %up_w.1, bf16[1,768,2048]{2,1,0:T(8,128)(2,1)} %down_w.1), custom_call_target="tpu_custom_call" | custom-call | tf_op jit(solution)/shard_map/pallas_call | solution.py:284
  28.2 1.7 %copy.9 = bf16[72,2048]{1,0:T(8,128)(2,1)} copy(bf16[72,2048]{1,0:T(8,128)(2,1)} %shard_map.73) | data formatting | bytes 589824

commit v2 on v1

--- a/solution.py
+++ b/solution.py
@@ -11,6 +11,7 @@
 LANES = 128
 SUB = 8
 GROUP = 8
+VMEM_BYTES = 67043328
 
 
 def loop(count, body):
@@ -23,14 +24,17 @@
 def kernel(
     n,
     tokens,
-    gain,
-    chosen,
-    route,
+    gain_h,
+    chosen_h,
+    route_h,
     gate_w,
     up_w,
     down_w,
     mixed,
     tok,
+    gain,
+    chosen,
+    route,
     wg,
     wu,
     wd,
@@ -90,15 +94,23 @@
     base = pl.multiple_of(core * half_rows, 8)
     load_tok = pltpu.make_async_copy(tokens.at[pl.ds(base, half_rows)], tok, load_sem.at[0])
     load_tok.start()
+    small = [
+        pltpu.make_async_copy(src, dst, load_sem.at[i + 4])
+        for i, (src, dst) in enumerate(((gain_h, gain), (chosen_h, chosen), (route_h, route)))
+    ]
+    for load in small:
+        load.start()
     loads = [
         pltpu.make_async_copy(src.at[0], dst, load_sem.at[i + 1])
         for i, (src, dst) in enumerate(((gate_w, wg), (up_w, wu), (down_w, wd)))
     ]
     for load in loads:
         load.start()
+    for load in small:
+        load.wait()
     load_tok.wait()
 
-    g = gain[...].astype(jnp.float32)
+    g = gain[...].astype(jnp.float32).reshape(1, width)
     values = tok[...].astype(jnp.float32)
     scale = lax.rsqrt(jnp.mean(values * values, axis=-1, keepdims=True) + 1e-06)
     normed[...] = (values * scale * g).astype(jnp.bfloat16)
@@ -280,43 +292,48 @@
     packed = pltpu.VMEM((chunks, rows, SUB, LANES), bf16)
     partial = pltpu.VMEM((chunks, blocks, block, cols), bf16)
     vmem = pl.BlockSpec(memory_space=pltpu.VMEM)
-    hbm = pl.BlockSpec(memory_space=pl.ANY)
+    hbm = pl.BlockSpec(memory_space=pltpu.HBM)
+    scratch = [
+        pltpu.VMEM((half_rows, width), bf16),
+        pltpu.VMEM(norm_gain.shape, norm_gain.dtype),
+        pltpu.VMEM(chosen_rows.shape, chosen_rows.dtype),
+        pltpu.VMEM(route_weights.shape, route_weights.dtype),
+        pltpu.VMEM(gate_weight.shape[1:], bf16),
+        pltpu.VMEM(up_weight.shape[1:], bf16),
+        pltpu.VMEM(down_weight.shape[1:], bf16),
+        pltpu.VMEM((half_rows, width), bf16),
+        packed,
+        packed,
+        packed,
+        pltpu.VMEM((2 * block * SUB, LANES), f32),
+        pltpu.VMEM((2 * block, cols), bf16),
+        pltpu.VMEM((blocks, 2 * block, ff), f32),
+        pltpu.VMEM((blocks, 2 * block, ff), f32),
+        pltpu.VMEM((blocks, 2 * block, ff), bf16),
+        partial,
+        partial,
+        partial,
+        packed,
+        packed,
+        pltpu.VMEM((rows, half_rows), f32),
+        pltpu.VMEM((rows, half_rows), f32),
+        pltpu.VMEM((rows, cols), f32),
+    ]
+    limit = VMEM_BYTES - half_rows * width * 2
     return pl.pallas_call(
         functools.partial(kernel, n),
         out_shape=jax.ShapeDtypeStruct((half_rows, width), bf16),
-        in_specs=[hbm, vmem, vmem, vmem, hbm, hbm, hbm],
+        in_specs=[hbm] * 7,
         out_specs=vmem,
-        scratch_shapes=[
-            pltpu.VMEM((half_rows, width), bf16),
-            pltpu.VMEM(gate_weight.shape[1:], bf16),
-            pltpu.VMEM(up_weight.shape[1:], bf16),
-            pltpu.VMEM(down_weight.shape[1:], bf16),
-            pltpu.VMEM((half_rows, width), bf16),
-            packed,
-            packed,
-            packed,
-            pltpu.VMEM((2 * block * SUB, LANES), f32),
-            pltpu.VMEM((2 * block, cols), bf16),
-            pltpu.VMEM((blocks, 2 * block, ff), f32),
-            pltpu.VMEM((blocks, 2 * block, ff), f32),
-            pltpu.VMEM((blocks, 2 * block, ff), bf16),
-            partial,
-            partial,
-            partial,
-            packed,
-            packed,
-            pltpu.VMEM((rows, half_rows), f32),
-            pltpu.VMEM((rows, half_rows), f32),
-            pltpu.VMEM((rows, cols), f32),
-            pltpu.SemaphoreType.DMA((4,)),
-        ]
+        scratch_shapes=scratch
+        + [pltpu.SemaphoreType.DMA((7,))]
         + [pltpu.SemaphoreType.DMA((chunks,))] * 8,
         compiler_params=pltpu.CompilerParams(
-            collective_id=0, has_side_effects=True, vmem_limit_bytes=60 * 1024 * 1024
+            collective_id=0, has_side_effects=True, vmem_limit_bytes=limit
         ),
     )(
         tokens,
-        norm_gain.reshape(1, width),
+        norm_gain,
         chosen_rows,
         route_weights,
         gate_weight,

time: 30.1 us -> 28 us (0.930)
  local copies, waits for them, and re-layouts: 2.98 us -> 1.69 us
  Pallas kernels: 26.9 us -> 26.2 us
    reshape x1 -> x0, local copies, waits for them, and re-layouts: 1.29 us -> none  [local(): norm_gain.reshape(1, width)]
    pallas_call x1, Pallas kernels: 26.9 us -> 26.2 us  [local(): pl.pallas_call(functools.partial(kernel, n), out_shape=jax.ShapeDtypeStru...]
where the time goes in v2:
time: 28 us; the launch traced here: 27.9 us
  Pallas kernels  26.2 us (94%)
  local copies, waits for them, and re-layouts  1.69 us (6%)
    pallas_call x1, Pallas kernels, local(): pl.pallas_call(functools.partial(kernel, n), out_shape=jax.ShapeDtypeStru...  26.2 us
    unnamed x1, local copies, waits for them, and re-layouts  1.69 us

profile of v2, /device:TPU:0, one launch (start us, length us, event | category | flops | bytes accessed | tf_op | source)
XLA Modules:
  0.0 27.9 jit_solution(6639695577380540932)
XLA Ops:
  0.0 26.2 %shard_map.73 = bf16[72,2048]{1,0:T(8,128)(2,1)} custom-call(bf16[144,2048]{1,0:T(8,128)(2,1)} %tokens.1, bf16[2048]{0:T(1024)(128)(2,1)} %gain_h.1, s32[8,18]{1,0:T(8,128)} %chosen_h.1, f32[8,18]{1,0:T(8,128)} %route_h.1, bf16[1,2048,768]{2,1,0:T(8,128)(2,1)} %gate_w.1, bf16[1,2048,768]{2,1,0:T(8,128)(2,1)} %up_w.1, bf16[1,768,2048]{2,1,0:T(8,128)(2,1)} %down_w.1), custom_call_target="tpu_custom_call" | custom-call | tf_op jit(solution)/shard_map/pallas_call | solution.py:323
  26.2 1.7 %copy.9 = bf16[72,2048]{1,0:T(8,128)(2,1)} copy(bf16[72,2048]{1,0:T(8,128)(2,1)} %shard_map.73) | data formatting | bytes 589824

commit v3 on v2

--- a/solution.py
+++ b/solution.py
@@ -322,7 +322,7 @@
     limit = VMEM_BYTES - half_rows * width * 2
     return pl.pallas_call(
         functools.partial(kernel, n),
-        out_shape=jax.ShapeDtypeStruct((half_rows, width), bf16),
+        out_shape=pltpu.VMEM((half_rows, width), bf16),
         in_specs=[hbm] * 7,
         out_specs=vmem,
         scratch_shapes=scratch

time: 28 us -> 26.3 us (0.939)
  local copies, waits for them, and re-layouts: 1.69 us -> 0.72 us
  Pallas kernels: 26.2 us -> 25.5 us
    unnamed x1, local copies, waits for them, and re-layouts: 1.69 us -> 0.72 us
    pallas_call x1, Pallas kernels: 26.2 us -> 25.5 us  [local(): pl.pallas_call(functools.partial(kernel, n), out_shape=pltpu.VMEM((half_r...]
where the time goes in v3:
time: 26.3 us; the launch traced here: 26.2 us
  Pallas kernels  25.5 us (97%)
  local copies, waits for them, and re-layouts  0.72 us (3%)
    pallas_call x1, Pallas kernels, local(): pl.pallas_call(functools.partial(kernel, n), out_shape=pltpu.VMEM((half_r...  25.5 us
    unnamed x1, local copies, waits for them, and re-layouts  0.72 us

profile of v3, /device:TPU:0, one launch (start us, length us, event | category | flops | bytes accessed | tf_op | source)
XLA Modules:
  0.0 26.2 jit_solution(8444565027250606100)
XLA Ops:
  0.0 25.5 %shard_map.73 = bf16[72,2048]{1,0:T(8,128)(2,1)S(1)} custom-call(bf16[144,2048]{1,0:T(8,128)(2,1)} %tokens.1, bf16[2048]{0:T(1024)(128)(2,1)} %gain_h.1, s32[8,18]{1,0:T(8,128)} %chosen_h.1, f32[8,18]{1,0:T(8,128)} %route_h.1, bf16[1,2048,768]{2,1,0:T(8,128)(2,1)} %gate_w.1, bf16[1,2048,768]{2,1,0:T(8,128)(2,1)} %up_w.1, bf16[1,768,2048]{2,1,0:T(8,128)(2,1)} %down_w.1), custom_call_target="tpu_custom_call" | custom-call | tf_op jit(solution)/shard_map/pallas_call | solution.py:323
  25.5 0.7 %copy.9 = bf16[72,2048]{1,0:T(8,128)(2,1)} copy(bf16[72,2048]{1,0:T(8,128)(2,1)S(1)} %shard_map.73) | data formatting | bytes 589824

commit v4 on v3

v4 whole, which is shorter than its diff:
```python
import functools

import jax
import jax.numpy as jnp
from jax import lax
from jax.experimental import pallas as pl
from jax.experimental.pallas import tpu as pltpu
from jax.sharding import PartitionSpec as P

MESH = pl.DeviceIdType.MESH
LANES = 128
SUB = 8
GROUP = 8
VMEM_BYTES = 67043328


def loop(count, body):
    if count == 1:
        body(0)
    else:
        lax.fori_loop(0, count, lambda i, carry: (body(i), carry)[1], 0)


def group_sizes(half):
    return [half - half // 2, half // 2]


def kernel(
    n,
    tokens,
    gain_h,
    chosen_h,
    route_h,
    gate_w,
    up_w,
    down_w,
    mixed,
    tok,
    gain,
    chosen,
    route,
    wg,
    wu,
    wd,
    normed,
    out_x,
    in_x,
    sib_x,
    flat,
    x_cols,
    hidden,
    p_send,
    p_recv,
    p_own,
    c_send,
    c_recv,
    g_rows,
    w_rows,
    r_cols,
    load_sem,
    d_send,
    d_recv,
    f_send,
    f_recv,
    q_send,
    q_recv,
    b_send,
    b_recv,
):
    half_rows, width = tok.shape
    experts, slots = chosen.shape
    half = slots // 2
    sizes = group_sizes(half)
    starts = [sum(sizes[:j]) for j in range(len(sizes))]
    blocks = experts // GROUP
    pieces = width // LANES
    cols = width // 2
    me = lax.axis_index("ep")
    core = lax.axis_index("tp")
    sib = {"tp": 1 - core}

    def peer(i):
        return lax.rem(me + i, n)

    barrier = pltpu.get_barrier_semaphore()
    pl.semaphore_signal(barrier, inc=1, device_id=sib, device_id_type=MESH)
    lax.fori_loop(
        1,
        n,
        lambda i, c: (
            pl.semaphore_signal(barrier, inc=1, device_id={"ep": peer(i)}, device_id_type=MESH),
            c,
        )[1],
        0,
    )
    base = pl.multiple_of(core * half_rows, 8)
    load_tok = pltpu.make_async_copy(tokens.at[pl.ds(base, half_rows)], tok, load_sem.at[0])
    load_tok.start()
    small = [
        pltpu.make_async_copy(src, dst, load_sem.at[i + 4])
        for i, (src, dst) in enumerate(((gain_h, gain), (chosen_h, chosen), (route_h, route)))
    ]
    for load in small:
        load.start()
    loads = [
        pltpu.make_async_copy(src.at[0], dst, load_sem.at[i + 1])
        for i, (src, dst) in enumerate(((gate_w, wg), (up_w, wu), (down_w, wd)))
    ]
    for load in small:
        load.wait()
    first = me * (2 * half_rows) + core * half_rows
    picked = (chosen[...] - first).astype(jnp.float32).T
    weight = route[...].T
    lane = lax.broadcasted_iota(jnp.int32, (half, half_rows), 1).astype(jnp.float32)
    for e in range(experts):
        pair = [picked[h * half : (h + 1) * half, e : e + 1] for h in range(2)]
        row = jnp.where(core == 0, pair[0], pair[1])
        pair = [weight[h * half : (h + 1) * half, e : e + 1] for h in range(2)]
        share = jnp.where(core == 0, pair[0], pair[1])
        here = lane == row
        for j, size in enumerate(sizes):
            here_j = slice(starts[j], starts[j] + size)
            at = slice(experts * starts[j] + e * size, experts * starts[j] + (e + 1) * size)
            g_rows[at, :] = jnp.where(here, 1.0, 0.0)[here_j]
            w_rows[at, :] = jnp.where(here, share, 0.0)[here_j]

    load_tok.wait()
    for load in loads:
        load.start()

    g = gain[...].astype(jnp.float32).reshape(1, width)
    values = tok[...].astype(jnp.float32)
    scale = lax.rsqrt(jnp.mean(values * values, axis=-1, keepdims=True) + 1e-06)
    normed[...] = (values * scale * g).astype(jnp.bfloat16)

    def rows_of(j, b):
        block = GROUP * sizes[j]
        at = b * block
        return pl.ds(at if isinstance(b, int) else pl.multiple_of(at, 8), block)

    def total_rows(j, b):
        block = GROUP * sizes[j]
        at = experts * starts[j] + b * block
        return pl.ds(at if isinstance(b, int) else pl.multiple_of(at, 8), block)

    def pack(value, ref, j, b):
        block = GROUP * sizes[j]
        for s in range(pieces):
            flat[pl.ds(s, block, stride=pieces), :] = value[:, s * LANES : (s + 1) * LANES]
        packed = flat[: block * pieces, :].reshape(block, pieces, LANES)
        ref[j, rows_of(j, b)] = packed.astype(jnp.bfloat16)

    def gather(j):
        def one(b):
            hot = g_rows[total_rows(j, b), :].astype(jnp.bfloat16)
            got = jnp.dot(hot, normed[...], preferred_element_type=jnp.float32)
            pack(got, out_x, j, b)

        loop(blocks, one)

    def mine(ref, j, e):
        return ref.at[j, pl.ds(e * sizes[j], sizes[j])]

    def exchange(src, dst, j, send_sem, recv_sem):
        def one(i, c):
            e = peer(i)
            pltpu.make_async_remote_copy(
                src_ref=mine(src, j, e),
                dst_ref=mine(dst, j, me),
                send_sem=send_sem.at[j],
                recv_sem=recv_sem.at[j],
                device_id={"ep": e},
                device_id_type=MESH,
            ).start()
            return c

        lax.fori_loop(1, n, one, 0)
        for r in range(sizes[j]):
            dst[j, me * sizes[j] + r] = src[j, me * sizes[j] + r]

    def all_of(src, dst, j, send_sem, recv_sem):
        part = pl.ds(0, (n - 1) * sizes[j])
        return pltpu.make_async_remote_copy(
            src_ref=src.at[j, part],
            dst_ref=dst.at[j, part],
            send_sem=send_sem.at[j],
            recv_sem=recv_sem.at[j],
            device_id=sib,
            device_id_type=MESH,
        )

    def forward(j):
        part = pl.ds(0, n * sizes[j])
        return pltpu.make_async_remote_copy(
            src_ref=in_x.at[j, part],
            dst_ref=sib_x.at[j, part],
            send_sem=f_send.at[j],
            recv_sem=f_recv.at[j],
            device_id=sib,
            device_id_type=MESH,
        )

    def swap(j, k):
        part = pl.ds(0, n * sizes[j])
        return pltpu.make_async_remote_copy(
            src_ref=p_send.at[j, k, part],
            dst_ref=p_recv.at[j, k, part],
            send_sem=q_send.at[2 * j + k],
            recv_sem=q_recv.at[2 * j + k],
            device_id=sib,
            device_id_type=MESH,
        )

    groups = range(len(sizes))
    gather(0)
    pl.semaphore_wait(barrier, n)
    exchange(out_x, in_x, 0, d_send, d_recv)
    for j in groups[1:]:
        gather(j)
        exchange(out_x, in_x, j, d_send, d_recv)

    def arrive(j):
        all_of(out_x, in_x, j, d_send, d_recv).wait_recv()
        forward(j).start()

    def compute(j):
        block = GROUP * sizes[j]

        def project(b):
            for h, ref in enumerate((in_x, sib_x)):
                got = ref[j, rows_of(j, b)].astype(jnp.float32)
                flat[pl.ds(h * block * pieces, block * pieces), :] = got.reshape(
                    block * pieces, LANES
                )
            for s in range(pieces):
                x_cols[: 2 * block, s * LANES : (s + 1) * LANES] = flat[
                    pl.ds(s, 2 * block, stride=pieces), :
                ].astype(jnp.bfloat16)
            x = x_cols[: 2 * block, :]
            gate = jnp.dot(x, wg[...], preferred_element_type=jnp.float32)
            up = jnp.dot(x, wu[...], preferred_element_type=jnp.float32)
            act = (gate / (1.0 + jnp.exp(-gate)) * up).astype(jnp.bfloat16)
            hidden[b, : 2 * block, :] = act

        loop(blocks, project)
        if j == 0:
            loads[2].wait()
        for k in range(2):

            def down(b):
                part = jnp.dot(
                    hidden[b, : 2 * block, :],
                    wd[:, k * cols : (k + 1) * cols],
                    preferred_element_type=jnp.float32,
                )
                p_own[j, k, rows_of(j, b)] = part[:block].astype(jnp.bfloat16)
                p_send[j, k, rows_of(j, b)] = part[block:].astype(jnp.bfloat16)

            loop(blocks, down)
            swap(j, k).start()

    def give(j):
        for k in range(2):
            swap(j, k).wait_recv()

        def combine(b):
            both = [
                p_own[j, k, rows_of(j, b)].astype(jnp.float32)
                + p_recv[j, k, rows_of(j, b)].astype(jnp.float32)
                for k in range(2)
            ]
            pack(jnp.concatenate(both, axis=1), c_send, j, b)

        loop(blocks, combine)
        exchange(c_send, c_recv, j, b_send, b_recv)

    arrive(0)
    for load in loads[:2]:
        load.wait()
    for j in groups:
        forward(j).wait_recv()
        compute(j)
        if j + 1 < len(sizes):
            arrive(j + 1)
        give(j)

    spread = w_rows[...].T
    high = spread.astype(jnp.bfloat16)
    low = (spread - high.astype(jnp.float32)).astype(jnp.bfloat16)
    for j in groups:
        all_of(c_send, c_recv, j, b_send, b_recv).wait_recv()
        block = GROUP * sizes[j]

        def unpack(b):
            got = c_recv[j, rows_of(j, b)].astype(jnp.float32)
            flat[: block * pieces, :] = got.reshape(block * pieces, LANES)
            for s in range(pieces):
                r_cols[total_rows(j, b), s * LANES : (s + 1) * LANES] = flat[
                    pl.ds(s, block, stride=pieces), :
                ]

        loop(blocks, unpack)
    for k in range(2):
        part = slice(k * cols, (k + 1) * cols)
        res = r_cols[:, part].astype(jnp.bfloat16)
        total = jnp.dot(high, res, preferred_element_type=jnp.float32)
        total = total + jnp.dot(low, res, preferred_element_type=jnp.float32)
        mixed[:, part] = total.astype(jnp.bfloat16)

    for j in groups:
        all_of(out_x, in_x, j, d_send, d_recv).wait_send()
        forward(j).wait_send()
        for k in range(2):
            swap(j, k).wait_send()
        all_of(c_send, c_recv, j, b_send, b_recv).wait_send()


def local(n, tokens, norm_gain, chosen_rows, route_weights, gate_weight, up_weight, down_weight):
    tok_rows, width = tokens.shape
    half_rows = tok_rows // 2
    experts, slots = chosen_rows.shape
    half = slots // 2
    rows = experts * half
    sizes = group_sizes(half)
    top = max(sizes)
    block = GROUP * top
    pieces = width // LANES
    ff = gate_weight.shape[2]
    bf16, f32 = jnp.bfloat16, jnp.float32
    packed = pltpu.VMEM((len(sizes), experts * top, pieces, LANES), bf16)
    partial = pltpu.VMEM((len(sizes), 2, experts * top, width // 2), bf16)
    vmem = pl.BlockSpec(memory_space=pltpu.VMEM)
    hbm = pl.BlockSpec(memory_space=pltpu.HBM)
    scratch = [
        pltpu.VMEM((half_rows, width), bf16),
        pltpu.VMEM(norm_gain.shape, norm_gain.dtype),
        pltpu.VMEM(chosen_rows.shape, chosen_rows.dtype),
        pltpu.VMEM(route_weights.shape, route_weights.dtype),
        pltpu.VMEM(gate_weight.shape[1:], bf16),
        pltpu.VMEM(up_weight.shape[1:], bf16),
        pltpu.VMEM(down_weight.shape[1:], bf16),
        pltpu.VMEM((half_rows, width), bf16),
        packed,
        packed,
        packed,
        pltpu.VMEM((2 * block * pieces, LANES), f32),
        pltpu.VMEM((2 * block, width), bf16),
        pltpu.VMEM((experts // GROUP, 2 * block, ff), bf16),
        partial,
        partial,
        partial,
        packed,
        packed,
        pltpu.VMEM((rows, half_rows), f32),
        pltpu.VMEM((rows, half_rows), f32),
        pltpu.VMEM((rows, width), f32),
    ]
    limit = VMEM_BYTES - half_rows * width * 2
    return pl.pallas_call(
        functools.partial(kernel, n),
        out_shape=pltpu.VMEM((half_rows, width), bf16),
        in_specs=[hbm] * 7,
        out_specs=vmem,
        scratch_shapes=scratch
        + [pltpu.SemaphoreType.DMA((7,))]
        + [pltpu.SemaphoreType.DMA((2 * len(sizes),))] * 8,
        compiler_params=pltpu.CompilerParams(
            collective_id=0, has_side_effects=True, vmem_limit_bytes=limit
        ),
    )(
        tokens,
        norm_gain,
        chosen_rows,
        route_weights,
        gate_weight,
        up_weight,
        down_weight,
    )


def solution(mesh):
    return jax.shard_map(
        functools.partial(local, mesh.shape["ep"]),
        mesh=mesh,
        in_specs=(
            P(("grp", "ep"), None),
            P(),
            P("grp", "ep"),
            P("grp", "ep"),
            P("ep", None, "tp"),
            P("ep", None, "tp"),
            P("ep", "tp", None),
        ),
        out_specs=P(("grp", "ep", "tp"), None),
        check_vma=False,
    )
```

time: 26.3 us -> 25.2 us (0.958)
  Pallas kernels: 25.5 us -> 24.2 us
    pallas_call x1, Pallas kernels: 25.5 us -> 24.2 us  [local(): pl.pallas_call(functools.partial(kernel, n), out_shape=pltpu.VMEM((half_r...]
where the time goes in v4:
time: 25.2 us; the launch traced here: 25 us
  Pallas kernels  24.2 us (96%)
  local copies, waits for them, and re-layouts  0.72 us (3%)
    pallas_call x1, Pallas kernels, local(): pl.pallas_call(functools.partial(kernel, n), out_shape=pltpu.VMEM((half_r...  24.2 us
    unnamed x1, local copies, waits for them, and re-layouts  0.72 us

profile of v4, /device:TPU:0, one launch (start us, length us, event | category | flops | bytes accessed | tf_op | source)
XLA Modules:
  0.0 25.0 jit_solution(11062217566070326195)
XLA Ops:
  0.0 24.2 %shard_map.73 = bf16[72,2048]{1,0:T(8,128)(2,1)S(1)} custom-call(bf16[144,2048]{1,0:T(8,128)(2,1)} %tokens.1, bf16[2048]{0:T(1024)(128)(2,1)} %gain_h.1, s32[8,18]{1,0:T(8,128)} %chosen_h.1, f32[8,18]{1,0:T(8,128)} %route_h.1, bf16[1,2048,768]{2,1,0:T(8,128)(2,1)} %gate_w.1, bf16[1,2048,768]{2,1,0:T(8,128)(2,1)} %up_w.1, bf16[1,768,2048]{2,1,0:T(8,128)(2,1)} %down_w.1), custom_call_target="tpu_custom_call" | custom-call | tf_op jit(solution)/shard_map/pallas_call | solution.py:359
  24.2 0.7 %copy.9 = bf16[72,2048]{1,0:T(8,128)(2,1)} copy(bf16[72,2048]{1,0:T(8,128)(2,1)S(1)} %shard_map.73) | data formatting | bytes 589824

commit v5 on v4

--- a/solution.py
+++ b/solution.py
@@ -22,7 +22,7 @@
 
 
 def group_sizes(half):
-    return [half - half // 2, half // 2]
+    return [half // 2, half - half // 2]
 
 
 def kernel(

time: 25.2 us -> 24.9 us (0.988)
  Pallas kernels: 24.2 us -> 23.9 us
    pallas_call x1, Pallas kernels: 24.2 us -> 23.9 us  [local(): pl.pallas_call(functools.partial(kernel, n), out_shape=pltpu.VMEM((half_r...]
where the time goes in v5:
time: 24.9 us; the launch traced here: 24.6 us
  Pallas kernels  23.9 us (96%)
  local copies, waits for them, and re-layouts  0.72 us (3%)
    pallas_call x1, Pallas kernels, local(): pl.pallas_call(functools.partial(kernel, n), out_shape=pltpu.VMEM((half_r...  23.9 us
    unnamed x1, local copies, waits for them, and re-layouts  0.72 us

profile of v5, /device:TPU:0, one launch (start us, length us, event | category | flops | bytes accessed | tf_op | source)
XLA Modules:
  0.0 24.6 jit_solution(7999714500178998200)
XLA Ops:
  0.0 23.9 %shard_map.73 = bf16[72,2048]{1,0:T(8,128)(2,1)S(1)} custom-call(bf16[144,2048]{1,0:T(8,128)(2,1)} %tokens.1, bf16[2048]{0:T(1024)(128)(2,1)} %gain_h.1, s32[8,18]{1,0:T(8,128)} %chosen_h.1, f32[8,18]{1,0:T(8,128)} %route_h.1, bf16[1,2048,768]{2,1,0:T(8,128)(2,1)} %gate_w.1, bf16[1,2048,768]{2,1,0:T(8,128)(2,1)} %up_w.1, bf16[1,768,2048]{2,1,0:T(8,128)(2,1)} %down_w.1), custom_call_target="tpu_custom_call" | custom-call | tf_op jit(solution)/shard_map/pallas_call | solution.py:359
  23.9 0.7 %copy.9 = bf16[72,2048]{1,0:T(8,128)(2,1)} copy(bf16[72,2048]{1,0:T(8,128)(2,1)S(1)} %shard_map.73) | data formatting | bytes 589824
